TPU v7x, 256 devices: a whole 4x4x8 slice. The times are simulated.
256 devices in a mesh: sp: 32 (over z, y), tp: 8 (over x, core).
Axes of the slice: x: 4, y: 4, z: 8, core: 2. Of those that a mesh axis runs over, the one named last changes fastest.
Arguments:
- hidden: bfloat16 [24576, 2048], P(('sp', 'tp')), may hold values from -6 to 6
- norm_gain: float32 [2, 2048], replicated, may hold values from 0.1 to 1.9
- w_value: bfloat16 [2, 2048, 2048], P(None, 'sp', 'tp'), may hold values from -0.125 to 0.125
- w_gate: bfloat16 [2, 2048, 2048], P(None, 'sp', 'tp'), may hold values from -0.125 to 0.125
- conv_weight: float32 [2, 31, 2048], P(None, None, 'tp'), may hold values from -3 to 3
- conv_bias: float32 [2, 2048], P(None, 'tp'), may hold values from -3 to 3
- chan_gain: float32 [2, 2048], P(None, 'tp'), may hold values from 0.1 to 1.9
- chan_shift: float32 [2, 2048], P(None, 'tp'), may hold values from -3 to 3
- w_out: bfloat16 [2, 2048, 2048], P(None, 'tp', 'sp'), may hold values from -0.125 to 0.125
Outputs:
- result: bfloat16 [24576, 2048], P(('sp', 'tp'))
All inputs are finite; a program needn't handle non-finite values.
Results may differ from a plain program's by a relative error of at most 0.015.
Values may be sent and summed in bfloat16 or wider, within the bound.
No kernel may reach another device: no remote copies, remote signals or barrier semaphores. Data moves between devices by JAX's collectives and lax.ppermute only.
A program may use at most 64 MiB of HBM per device.

v0:
```python
import jax
import jax.numpy as jnp
from jax import lax
from jax.sharding import Mesh
from jax.sharding import PartitionSpec as P

SP = ("sp_0", "sp_1")
SP_TP = ("sp_0", "sp_1", "tp")
EPS = 1e-06


def sent_together(arrays, axis, dim, along):
    widths = [a.shape[along] for a in arrays]
    both = jnp.concatenate(arrays, axis=along)
    whole = lax.all_gather(both, axis, axis=dim, tiled=True)
    return tuple(jnp.split(whole, [sum(widths[:k]) for k in range(1, len(widths))], axis=along))


def shifted(shard, axis, by):
    size = lax.axis_size(axis)
    pairs = [(i, i + by) for i in range(size) if 0 <= i + by < size]
    return lax.ppermute(shard, axis, pairs)


def sent_to_all(shard, axis):
    size = lax.axis_size(axis)
    return lax.all_to_all(
        jnp.broadcast_to(shard[None], (size, *shard.shape)), axis, 0, 0, tiled=True
    )


def of_everyone(shard, axis):
    everything = sent_to_all(shard, axis)
    return jnp.sum(everything, axis=0)


def together(arrays, axis):
    ravelled, at, finished = (jnp.concatenate([a.reshape(-1) for a in arrays]), 0, [])
    running = of_everyone(ravelled, axis)
    for a in arrays:
        finished.append(running[at : at + a.size].reshape(a.shape))
        at += a.size
    return tuple(finished)


def whole_of(shard, axes, dim):
    if not axes:
        return shard
    nearer = lax.all_gather(shard, axes[-1], axis=dim, tiled=True)
    return whole_of(nearer, axes[:-1], dim)


def cut_along(shard, dim, size):
    dims = shard.shape
    tiles = shard.reshape(*dims[:dim], size, dims[dim] // size, *dims[dim + 1 :])
    return jnp.moveaxis(tiles, dim, 0)


def sum_at_owner(shard, axis, dim):
    tiles = cut_along(shard, dim, lax.axis_size(axis))
    arrived = lax.all_to_all(tiles, axis, split_axis=0, concat_axis=0, tiled=True)
    return arrived.astype(jnp.float32).sum(axis=0)


def body(hidden, norm_gain, w_value, w_gate, conv_weight, conv_bias, chan_gain, chan_shift, w_out):
    group = lax.axis_size("tp")
    own_rows = hidden.shape[0]
    chans = w_value.shape[2]
    taps = conv_weight.shape[1]
    state = hidden
    for layer in range(norm_gain.shape[0]):
        xf = state.astype(jnp.float32)
        scale = lax.rsqrt(jnp.mean(xf * xf, axis=1, keepdims=True) + EPS)
        normed = (xf * scale * norm_gain[layer][None, :]).astype(jnp.bfloat16)
        tokens = lax.all_gather(normed, "tp", axis=0, tiled=True)
        empty = jnp.zeros((tokens.shape[0], chans), jnp.float32)

        def add_both(totals, pieces, start, tokens=tokens):
            return (
                jnp.dot(tokens, pieces[0], preferred_element_type=jnp.float32),
                jnp.dot(tokens, pieces[1], preferred_element_type=jnp.float32),
            )

        lin, gate = add_both(
            (empty, empty), sent_together((w_value[layer], w_gate[layer]), SP, 0, 1), jnp.int32(0)
        )
        glu = (lin * jax.nn.sigmoid(gate)).astype(jnp.bfloat16)
        before = shifted(glu[tokens.shape[0] - (taps - 1) :], SP, 1)
        window = jnp.concatenate([before, glu], axis=0).astype(jnp.float32)
        length = tokens.shape[0]
        mixed = jnp.zeros((length, chans), jnp.float32) + conv_bias[layer][None, :]
        for tap in range(taps):
            mixed = mixed + conv_weight[layer, tap][None, :] * window[tap : tap + length]
        totals = together((jnp.sum(mixed, axis=1), jnp.sum(mixed * mixed, axis=1)), "tp")
        mean = (totals[0] / (chans * group))[:, None]
        msq = (totals[1] / (chans * group))[:, None]
        var = msq - mean * mean
        act = jax.nn.silu(
            (mixed - mean) * lax.rsqrt(var + EPS) * chan_gain[layer][None, :]
            + chan_shift[layer][None, :]
        ).astype(jnp.bfloat16)

        def project(piece, start, act=act):
            return jnp.dot(act, piece, preferred_element_type=jnp.float32)

        partial_out = project(whole_of(w_out[layer], SP, 1), jnp.int32(0))

        def take_rows(start, count, partial_out=partial_out):
            return partial_out

        update = sum_at_owner(
            take_rows(jnp.int32(0), own_rows * lax.axis_size("tp")).astype(jnp.bfloat16), "tp", 0
        )
        state = (xf + update).astype(jnp.bfloat16)
    return state


def solution(mesh):
    torus = Mesh(mesh.devices.reshape(8, 4, mesh.shape["tp"]), ("sp_0", "sp_1", "tp"))
    in_specs = (
        P(SP_TP, None),
        P(),
        P(None, SP, "tp"),
        P(None, SP, "tp"),
        P(None, None, "tp"),
        P(None, "tp"),
        P(None, "tp"),
        P(None, "tp"),
        P(None, "tp", SP),
    )
    out_specs = P(SP_TP, None)
    return jax.shard_map(body, mesh=torus, in_specs=in_specs, out_specs=out_specs, check_vma=False)
```

profile of v0, /device:TPU:1, one launch (start us, length us, event | category | flops | bytes accessed | tf_op | source)
XLA Modules:
  0.0 361.9 jit_solution(7405386278213270947)
XLA Ops:
  8.1 1.2 fusion.14
  9.2 0.8 fusion.112
  10.1 1.9 fusion.16
  12.8 11.2 %all-gather = bf16[1,256,256]{1,2,0:T(8,128)(2,1)} all-gather(bf16[1,256,64]{1,2,0:T(8,128)(2,1)S(1)} %get-tuple-element.17), channel_id=2, replica_groups=mesh['sp_0'=8,'sp_1'=4,'tp'=8] {'sp_1'}, dimensions={2}, use_global_device_ids=true | all-gather | bytes 163840 | tf_op jit(solution)/shard_map/all_gather | solution.py:49
  24.7 0.9 fusion.110
  25.6 0.9 fusion.109
  28.0 59.0 %all-gather.13.cloned.1.call-done = bf16[2048,512]{1,0:T(8,128)(2,1)} async-done(((bf16[64,512]{1,0:T(8,128)(2,1)}), bf16[2048,512]{1,0:T(8,128)(2,1)}) %all-gather.13.cloned.1.call-update) | async-done | bytes 2097168 | tf_op jit(solution)/shard_map/all_gather | solution.py:15
  87.1 34.3 %all-gather.11.cloned.1.call-done = bf16[768,2048]{1,0:T(8,128)(2,1)} async-done(((bf16[96,2048]{1,0:T(8,128)(2,1)}), bf16[768,2048]{1,0:T(8,128)(2,1)}) %all-gather.11.cloned.1.call-update) | async-done | bytes 3145744 | tf_op jit(solution)/shard_map/all_gather | solution.py:75
  121.4 3.3 fusion.3
  124.7 1.0 fusion.6
  125.8 3.1 collective-permute-start
  128.9 0.8 collective-permute-done
  129.8 3.5 fusion.103
  134.0 4.4 %all-to-all-start = ((f32[8,1,1536]{2,1,0:T(1,128)}), f32[8,1,1536]{2,1,0:T(1,128)S(1)}, u32[]{:S(2)}, u32[]{:S(2)}) async-start(f32[8,1,1536]{2,1,0:T(1,128)} %broadcast_in_dim.4), calls=%async_computation | async-start | bytes 98304 | tf_op jit(solution)/shard_map/all_to_all | solution.py:27
  138.4 4.8 %all-to-all-done = f32[8,1,1536]{2,1,0:T(1,128)S(1)} async-done(((f32[8,1,1536]{2,1,0:T(1,128)}), f32[8,1,1536]{2,1,0:T(1,128)S(1)}, u32[]{:S(2)}, u32[]{:S(2)}) %all-to-all-start) | async-done | bytes 49184 | tf_op jit(solution)/shard_map/all_to_all | solution.py:27
  143.3 13.7 %all-gather.19.cloned.1.call-done = bf16[1,256,2048]{1,2,0:T(8,128)(2,1)} async-done(((bf16[1,256,256]{1,2,0:T(8,128)(2,1)}), bf16[1,256,2048]{1,2,0:T(8,128)(2,1)}) %all-gather.19.cloned.1.call-update) | async-done | bytes 1048592 | tf_op jit(solution)/shard_map/all_gather | solution.py:49
  156.9 2.3 convolution_convert_fusion.1
  159.3 46.4 %all_to_all.22 = bf16[8,96,2048]{2,1,0:T(8,128)(2,1)S(1)} all-to-all(bf16[8,96,2048]{2,1,0:T(8,128)(2,1)S(1)} %bitcast.90), channel_id=1, replica_groups=mesh['sp_0'=8,'sp_1'=4,'tp'=8] {'tp'}, dimensions={0} | all-to-all | bytes 6291456 | tf_op jit(solution)/shard_map/all_to_all | solution.py:61
  206.9 0.9 fusion.20
  207.9 11.0 %all-gather.2 = bf16[1,256,256]{1,2,0:T(8,128)(2,1)} all-gather(bf16[1,256,64]{1,2,0:T(8,128)(2,1)S(1)} %get-tuple-element.18), channel_id=4, replica_groups=mesh['sp_0'=8,'sp_1'=4,'tp'=8] {'sp_1'}, dimensions={2}, use_global_device_ids=true | all-gather | bytes 163840 | tf_op jit(solution)/shard_map/all_gather | solution.py:49
  219.0 16.4 %all-gather.17.cloned.1.call-done = bf16[2048,512]{1,0:T(8,128)(2,1)} async-done(((bf16[64,512]{1,0:T(8,128)(2,1)}), bf16[2048,512]{1,0:T(8,128)(2,1)}) %all-gather.17.cloned.1.call-update) | async-done | bytes 2097168 | tf_op jit(solution)/shard_map/all_gather | solution.py:15
  235.4 34.2 %all-gather.15.cloned.1.call-done = bf16[768,2048]{1,0:T(8,128)(2,1)} async-done(((bf16[96,2048]{1,0:T(8,128)(2,1)}), bf16[768,2048]{1,0:T(8,128)(2,1)}) %all-gather.15.cloned.1.call-update) | async-done | bytes 3145744 | tf_op jit(solution)/shard_map/all_gather | solution.py:75
  269.6 3.3 fusion.5
  272.9 1.0 fusion.7
  273.9 3.1 collective-permute-start.1
  277.0 0.9 fusion.108
  278.0 3.5 fusion.102
  281.6 8.6 %all_to_all.23 = f32[8,1,1536]{2,1,0:T(1,128)S(1)} all-to-all(f32[8,1,1536]{2,1,0:T(1,128)S(1)} %broadcast_in_dim.5), channel_id=1, replica_groups=mesh['sp_0'=8,'sp_1'=4,'tp'=8] {'tp'}, dimensions={0} | all-to-all | bytes 98304 | tf_op jit(solution)/shard_map/all_to_all | solution.py:27
  290.3 13.9 %all-gather.21.cloned.1.call-done = bf16[1,256,2048]{1,2,0:T(8,128)(2,1)} async-done(((bf16[1,256,256]{1,2,0:T(8,128)(2,1)}), bf16[1,256,2048]{1,2,0:T(8,128)(2,1)}) %all-gather.21.cloned.1.call-update) | async-done | bytes 1048592 | tf_op jit(solution)/shard_map/all_gather | solution.py:49
  304.2 2.3 convolution_convert_fusion
  306.5 47.1 %all_to_all.24 = bf16[8,96,2048]{2,1,0:T(8,128)(2,1)S(1)} all-to-all(bf16[8,96,2048]{2,1,0:T(8,128)(2,1)S(1)} %bitcast.91), channel_id=1, replica_groups=mesh['sp_0'=8,'sp_1'=4,'tp'=8] {'tp'}, dimensions={0} | all-to-all | bytes 6291456 | tf_op jit(solution)/shard_map/all_to_all | solution.py:61
  354.2 0.8 fusion.21
  (52 shorter events, 7.4 us)
Async XLA Ops:
  6.5 80.5 %all-gather.13.cloned.1.call-start = ((), (), s32[]{:S(2)}) async-start(), calls=%async_computation.5 | async-start | bytes 2162688 | tf_op jit(solution)/shard_map/all_gather | solution.py:15
  8.0 113.4 %all-gather.11.cloned.1.call-start = ((), (), s32[]{:S(2)}) async-start(), calls=%async_computation.4 | async-start | bytes 3538944 | tf_op jit(solution)/shard_map/all_gather | solution.py:75
  12.0 144.9 %all-gather.19.cloned.1.call-start = ((), (), s32[]{:S(2)}) async-start(), calls=%async_computation.8 | async-start | bytes 1179648 | tf_op jit(solution)/shard_map/all_gather | solution.py:49
  24.0 211.3 %all-gather.17.cloned.1.call-start = ((), (), s32[]{:S(2)}) async-start(), calls=%async_computation.7 | async-start | bytes 2162688 | tf_op jit(solution)/shard_map/all_gather | solution.py:15
  87.1 37.6 %copy-start.6 = (bf16[2048,512]{1,0:T(8,128)(2,1)S(1)}, bf16[2048,512]{1,0:T(8,128)(2,1)}, u32[]{:S(2)}) copy-start(bf16[2048,512]{1,0:T(8,128)(2,1)} %all-gather.13.cloned.1.call-done) | copy-start | bytes 6291460
  121.4 3.3 copy-start.3
  124.7 4.2 %copy-start.1 = (f32[2,256]{1,0:T(2,128)S(1)}, f32[2,256]{1,0:T(2,128)}, u32[]{:S(2)}) copy-start(f32[2,256]{1,0:T(2,128)} %param.15) | copy-start | bytes 6148
  125.8 4.0 %collective-permute-start = (bf16[30,256]{1,0:T(8,128)(2,1)S(1)}, bf16[30,256]{1,0:T(8,128)(2,1)S(1)}, u32[]{:S(2)}, u32[]{:S(2)}) collective-permute-start(bf16[30,256]{1,0:T(8,128)(2,1)S(1)} %slice.576), channel_id=1, source_target_pairs={{0,8},{8,16},{16,24},{24,32},{32,40},{40,48},{48,56},{56,64},{64,7... | collective-permute-start | bytes 46088 | tf_op jit(solution)/shard_map/ppermute | solution.py:22
  129.8 8.6 %copy-start.2 = (f32[2,256]{1,0:T(2,128)S(1)}, f32[2,256]{1,0:T(2,128)}, u32[]{:S(2)}) copy-start(f32[2,256]{1,0:T(2,128)} %param.16) | copy-start | bytes 6148
  134.0 9.2 %all-to-all-start = ((f32[8,1,1536]{2,1,0:T(1,128)}), f32[8,1,1536]{2,1,0:T(1,128)S(1)}, u32[]{:S(2)}, u32[]{:S(2)}) async-start(f32[8,1,1536]{2,1,0:T(1,128)} %broadcast_in_dim.4), calls=%async_computation | async-start | bytes 98304 | tf_op jit(solution)/shard_map/all_to_all | solution.py:27
  138.4 131.2 %all-gather.15.cloned.1.call-start = ((), (), s32[]{:S(2)}) async-start(), calls=%async_computation.6 | async-start | bytes 3538944 | tf_op jit(solution)/shard_map/all_gather | solution.py:75
  205.7 1.0 copy-start
  207.8 96.4 %all-gather.21.cloned.1.call-start = ((), (), s32[]{:S(2)}) async-start(), calls=%async_computation.9 | async-start | bytes 1179648 | tf_op jit(solution)/shard_map/all_gather | solution.py:49
  235.4 37.5 %copy-start.5 = (bf16[2048,512]{1,0:T(8,128)(2,1)S(1)}, bf16[2048,512]{1,0:T(8,128)(2,1)}, u32[]{:S(2)}) copy-start(bf16[2048,512]{1,0:T(8,128)(2,1)} %all-gather.17.cloned.1.call-done) | copy-start | bytes 6291460
  269.6 3.3 copy-start.4
  273.9 4.0 %collective-permute-start.1 = (bf16[30,256]{1,0:T(8,128)(2,1)S(1)}, bf16[30,256]{1,0:T(8,128)(2,1)S(1)}, u32[]{:S(2)}, u32[]{:S(2)}) collective-permute-start(bf16[30,256]{1,0:T(8,128)(2,1)S(1)} %slice.610), channel_id=1, source_target_pairs={{0,8},{8,16},{16,24},{24,32},{32,40},{40,48},{48,56},{56,64},{64,7... | collective-permute-start | bytes 46088 | tf_op jit(solution)/shard_map/ppermute | solution.py:22
Sparse Core Ops, SparseCore 0:
  9.9 77.1 all-gather.12
  88.9 32.4 all-gather.10
  123.2 33.7 all-gather.18
  159.4 75.9 all-gather.16
  237.0 32.4 all-gather.14
  271.2 32.9 all-gather.20
where the time goes:
time: 363 us; the launch traced here: 362 us
  waiting for transfers between devices  177 us (49%)
  blocking collectives  124 us (34%)
  other arithmetic  14.7 us (4%)
  between operations  13.7 us (4%)
  matrix products  13.3 us (4%)
  starting transfers between devices  10.8 us (3%)
  local copies, waits for them, and re-layouts  7.75 us (2%)
    all_to_all x2, blocking collectives, sum_at_owner(): lax.all_to_all(tiles, axis, split_axis=0, concat_axis=0, tiled=True)  93.5 us
    all_gather x2, waiting for transfers between devices, sent_together(): whole = lax.all_gather(both, axis, axis=dim, tiled=True)  75.5 us
    all_gather x2, waiting for transfers between devices, body(): tokens = lax.all_gather(normed, 'tp', axis=0, tiled=True)  68.5 us
    all_gather x2, waiting for transfers between devices, whole_of(): nearer = lax.all_gather(shard, axes[-1], axis=dim, tiled=True)  27.6 us
    all_gather x2, blocking collectives, whole_of(): nearer = lax.all_gather(shard, axes[-1], axis=dim, tiled=True)  22.2 us
    all_to_all x1, blocking collectives, sent_to_all(): lax.all_to_all(jnp.broadcast_to(shard[None], (size, *shard.shape)), axis,...  8.63 us
  transfers between devices with their start and end apart: 9, of which 8 were waited for; matrix products, arithmetic and copies ran while one was open for 8% of the time, Pallas kernels for 0%

commit v1 on v0

--- a/solution.py
+++ b/solution.py
@@ -7,6 +7,14 @@
 SP = ("sp_0", "sp_1")
 SP_TP = ("sp_0", "sp_1", "tp")
 EPS = 1e-06
+
+
+def tiled_gather(value, axis, dim):
+    size = lax.axis_size(axis)
+    repeats = [size if d == dim else 1 for d in range(value.ndim)]
+    return lax.all_to_all(
+        jnp.tile(value, repeats), axis, split_axis=dim, concat_axis=dim, tiled=True
+    )
 
 
 def sent_together(arrays, axis, dim, along):
@@ -72,7 +80,7 @@
         xf = state.astype(jnp.float32)
         scale = lax.rsqrt(jnp.mean(xf * xf, axis=1, keepdims=True) + EPS)
         normed = (xf * scale * norm_gain[layer][None, :]).astype(jnp.bfloat16)
-        tokens = lax.all_gather(normed, "tp", axis=0, tiled=True)
+        tokens = tiled_gather(normed, "tp", 0)
         empty = jnp.zeros((tokens.shape[0], chans), jnp.float32)
 
         def add_both(totals, pieces, start, tokens=tokens):

time: 363 us -> 308 us (0.85)
  blocking collectives: 124 us -> 79 us
  waiting for transfers between devices: 177 us -> 140 us
  starting transfers between devices: 10.8 us -> 36.8 us
    all_gather x2 -> x0, waiting for transfers between devices: 68.5 us -> none  [body(): tokens = lax.all_gather(normed, 'tp', axis=0, tiled=True)]
    all_to_all x0 -> x3, waiting for transfers between devices: none -> 68.5 us  [the longest x1 36 us: sum_at_owner(): lax.all_to_all(tiles, axis, split_axis=0, concat_axis=0, tiled=True)]
    all_to_all x2 -> x1, blocking collectives: 93.5 us -> 47.2 us  [sum_at_owner(): lax.all_to_all(tiles, axis, split_axis=0, concat_axis=0, tiled=True)]
    all_gather x2, waiting for transfers between devices: 75.5 us -> 46.5 us  [sent_together(): whole = lax.all_gather(both, axis, axis=dim, tiled=True)]
    all_to_all x0 -> x3, starting transfers between devices: none -> 21.4 us  [the longest x2 11.4 us: tiled_gather(): lax.all_to_all(jnp.tile(value, repeats), axis, split_axis=dim, concat_axi...]
    all_gather x2, waiting for transfers between devices: 27.6 us -> 20.6 us  [whole_of(): nearer = lax.all_gather(shard, axes[-1], axis=dim, tiled=True)]
    all_to_all x1, starting transfers between devices: 4.37 us -> 9.89 us  [sent_to_all(): lax.all_to_all(jnp.broadcast_to(shard[None], (size, *shard.shape)), axis,...]
    another operation x0 -> x2, local copies, waits for them, and re-layouts: none -> 4.06 us  [tiled_gather(): jnp.tile(value, repeats)]
  transfers between devices with their start and end apart: 9 -> 10, of which waited for: 8 -> 9; matrix products, arithmetic and copies ran while one was open for 8% -> 9% of each run, Pallas kernels for 0% -> 0%
where the time goes in v1:
time: 308 us
  waiting for transfers between devices  140 us (45%)
  blocking collectives  79 us (26%)
  starting transfers between devices  36.8 us (12%)
  other arithmetic  14.1 us (5%)
  between operations  13.6 us (4%)
  matrix products  13 us (4%)
  local copies, waits for them, and re-layouts  11 us (4%)
    all_to_all x1, blocking collectives, sum_at_owner(): lax.all_to_all(tiles, axis, split_axis=0, concat_axis=0, tiled=True)  47.2 us
    all_gather x2, waiting for transfers between devices, sent_together(): whole = lax.all_gather(both, axis, axis=dim, tiled=True)  46.5 us
    all_to_all x1, waiting for transfers between devices, sum_at_owner(): lax.all_to_all(tiles, axis, split_axis=0, concat_axis=0, tiled=True)  36 us
    all_to_all x2, waiting for transfers between devices, tiled_gather(): lax.all_to_all(jnp.tile(value, repeats), axis, split_axis=dim, concat_axi...  32.5 us
    all_gather x2, blocking collectives, whole_of(): nearer = lax.all_gather(shard, axes[-1], axis=dim, tiled=True)  22.9 us
    all_gather x2, waiting for transfers between devices, whole_of(): nearer = lax.all_gather(shard, axes[-1], axis=dim, tiled=True)  20.6 us
    all_to_all x2, starting transfers between devices, tiled_gather(): lax.all_to_all(jnp.tile(value, repeats), axis, split_axis=dim, concat_axi...  11.4 us
    all_to_all x1, starting transfers between devices, sum_at_owner(): lax.all_to_all(tiles, axis, split_axis=0, concat_axis=0, tiled=True)  9.95 us
  transfers between devices with their start and end apart: 10, of which 9 were waited for; matrix products, arithmetic and copies ran while one was open for 9% of the time, Pallas kernels for 0%

profile of v1, /device:TPU:1, one launch (start us, length us, event | category | flops | bytes accessed | tf_op | source)
XLA Modules:
  0.0 307.5 jit_solution(8900195166534772395)
XLA Ops:
  6.5 1.4 slice_bitcast_fusion
  8.6 1.2 fusion.14
  10.6 1.2 fusion.16
  11.8 2.0 tile.4
  13.8 6.9 %all-to-all-start = ((bf16[8,96,2048]{2,1,0:T(8,128)(2,1)}), bf16[8,96,2048]{2,1,0:T(8,128)(2,1)S(1)}, u32[]{:S(2)}, u32[]{:S(2)}) async-start(bf16[8,96,2048]{2,1,0:T(8,128)(2,1)} %tile.4), calls=%async_computation | async-start | bytes 6291456 | tf_op jit(solution)/shard_map/all_to_all | solution.py:15
  21.4 10.5 %all-gather = bf16[1,256,256]{1,2,0:T(8,128)(2,1)} all-gather(bf16[1,256,64]{1,2,0:T(8,128)(2,1)S(1)} %get-tuple-element.17), channel_id=2, replica_groups=mesh['sp_0'=8,'sp_1'=4,'tp'=8] {'sp_1'}, dimensions={2}, use_global_device_ids=true | all-gather | bytes 163840 | tf_op jit(solution)/shard_map/all_gather | solution.py:57
  33.1 25.1 %all-to-all-done = bf16[8,96,2048]{2,1,0:T(8,128)(2,1)S(1)} async-done(((bf16[8,96,2048]{2,1,0:T(8,128)(2,1)}), bf16[8,96,2048]{2,1,0:T(8,128)(2,1)S(1)}, u32[]{:S(2)}, u32[]{:S(2)}) %all-to-all-start) | async-done | bytes 3145760 | tf_op jit(solution)/shard_map/all_to_all | solution.py:15
  58.2 28.9 %all-gather.9.cloned.1.call-done = bf16[2048,512]{1,0:T(8,128)(2,1)} async-done(((bf16[64,512]{1,0:T(8,128)(2,1)}), bf16[2048,512]{1,0:T(8,128)(2,1)}) %all-gather.9.cloned.1.call-update) | async-done | bytes 2097168 | tf_op jit(solution)/shard_map/all_gather | solution.py:23
  87.1 2.4 fusion.3
  89.5 1.0 fusion.6
  90.5 2.4 collective-permute-start
  93.9 3.5 %fusion.103 = (f32[768]{0:T(1024)S(1)}, f32[768]{0:T(1024)S(1)}, f32[768,256]{1,0:T(8,128)S(1)}) fusion(f32[798,256]{1,0:T(8,128)S(1)} %maximum_convert_fusion, f32[256]{0:T(256)S(1)} %bitcast.134, f32[256]{0:T(256)S(1)} %bitcast.135, f32[256]{0:T(256)S(1)} %bitcast.136, f32[256]{0:T(256)S(1)} %bitcast.137, f32[256]{0:T(256)S(1)} %bitcast.138, ...), kind=kLoop, calls=%fused_computation.199 | loop fusion | flops 12777984 | bytes 25204736 | tf_op jit(solution)/shard_map/reduce_sum | solution.py:102
  98.0 9.9 %all-to-all-start.1 = ((f32[8,1,1536]{2,1,0:T(1,128)}), f32[8,1,1536]{2,1,0:T(1,128)S(1)}, u32[]{:S(2)}, u32[]{:S(2)}) async-start(f32[8,1,1536]{2,1,0:T(1,128)} %broadcast_in_dim.4), calls=%async_computation.1 | async-start | bytes 98304 | tf_op jit(solution)/shard_map/all_to_all | solution.py:35
  108.5 4.2 %all-to-all-done.1 = f32[8,1,1536]{2,1,0:T(1,128)S(1)} async-done(((f32[8,1,1536]{2,1,0:T(1,128)}), f32[8,1,1536]{2,1,0:T(1,128)S(1)}, u32[]{:S(2)}, u32[]{:S(2)}) %all-to-all-start.1) | async-done | bytes 49184 | tf_op jit(solution)/shard_map/all_to_all | solution.py:35
  112.8 11.4 %all-gather.13.cloned.1.call-done = bf16[1,256,2048]{1,2,0:T(8,128)(2,1)} async-done(((bf16[1,256,256]{1,2,0:T(8,128)(2,1)}), bf16[1,256,2048]{1,2,0:T(8,128)(2,1)}) %all-gather.13.cloned.1.call-update) | async-done | bytes 1048592 | tf_op jit(solution)/shard_map/all_gather | solution.py:57
  124.2 4.0 %convolution_convert_fusion.1 = bf16[768,2048]{1,0:T(8,128)(2,1)} fusion(bf16[1,256,2048]{1,2,0:T(8,128)(2,1)} %all-gather.13.cloned.1.call-done, f32[768,256]{1,0:T(8,128)S(1)} %get-tuple-element.12, f32[256]{0:T(256)S(1)} %bitcast.167, f32[256]{0:T(256)S(1)} %bitcast.166, f32[768]{0:T(1024)S(1)} %get-tuple-element.86, f32[768]{0:T(1024)S(1)} %get-tuple-element.85), kind=kOutput, calls=%fused_computation.3 | convolution fusion | flops 808648704 | bytes 4988928 | tf_op jit(solution)/shard_map/dot_general | solution.py:112
  128.1 10.0 %all-to-all-start.2 = ((bf16[8,96,2048]{2,1,0:T(8,128)(2,1)}), bf16[8,96,2048]{2,1,0:T(8,128)(2,1)S(1)}, u32[]{:S(2)}, u32[]{:S(2)}) async-start(bf16[8,96,2048]{2,1,0:T(8,128)(2,1)} %bitcast.96), calls=%async_computation.2 | async-start | bytes 6291456 | tf_op jit(solution)/shard_map/all_to_all | solution.py:69
  138.1 1.5 pad_maximum_fusion.1
  139.6 36.0 %all-to-all-done.2 = bf16[8,96,2048]{2,1,0:T(8,128)(2,1)S(1)} async-done(((bf16[8,96,2048]{2,1,0:T(8,128)(2,1)}), bf16[8,96,2048]{2,1,0:T(8,128)(2,1)S(1)}, u32[]{:S(2)}, u32[]{:S(2)}) %all-to-all-start.2) | async-done | bytes 3145760 | tf_op jit(solution)/shard_map/all_to_all | solution.py:69
  176.5 2.0 tile.5
  178.5 4.5 %all-to-all-start.3 = ((bf16[8,96,2048]{2,1,0:T(8,128)(2,1)}), bf16[8,96,2048]{2,1,0:T(8,128)(2,1)S(1)}, u32[]{:S(2)}, u32[]{:S(2)}) async-start(bf16[8,96,2048]{2,1,0:T(8,128)(2,1)} %tile.5), calls=%async_computation.3 | async-start | bytes 6291456 | tf_op jit(solution)/shard_map/all_to_all | solution.py:15
  183.0 12.4 %all-gather.2 = bf16[1,256,256]{1,2,0:T(8,128)(2,1)} all-gather(bf16[1,256,64]{1,2,0:T(8,128)(2,1)} %get-tuple-element.18), channel_id=4, replica_groups=mesh['sp_0'=8,'sp_1'=4,'tp'=8] {'sp_1'}, dimensions={2}, use_global_device_ids=true | all-gather | bytes 163840 | tf_op jit(solution)/shard_map/all_gather | solution.py:57
  195.4 17.6 %all-gather.11.cloned.1.call-done = bf16[2048,512]{1,0:T(8,128)(2,1)} async-done(((bf16[64,512]{1,0:T(8,128)(2,1)}), bf16[2048,512]{1,0:T(8,128)(2,1)}) %all-gather.11.cloned.1.call-update) | async-done | bytes 2097168 | tf_op jit(solution)/shard_map/all_gather | solution.py:23
  213.0 7.5 %all-to-all-done.3 = bf16[8,96,2048]{2,1,0:T(8,128)(2,1)S(1)} async-done(((bf16[8,96,2048]{2,1,0:T(8,128)(2,1)}), bf16[8,96,2048]{2,1,0:T(8,128)(2,1)S(1)}, u32[]{:S(2)}, u32[]{:S(2)}) %all-to-all-start.3) | async-done | bytes 3145760 | tf_op jit(solution)/shard_map/all_to_all | solution.py:15
  220.5 2.4 fusion.5
  223.0 1.0 fusion.7
  224.0 3.1 %collective-permute-start.1 = (bf16[30,256]{1,0:T(8,128)(2,1)S(1)}, bf16[30,256]{1,0:T(8,128)(2,1)S(1)}, u32[]{:S(2)}, u32[]{:S(2)}) collective-permute-start(bf16[30,256]{1,0:T(8,128)(2,1)S(1)} %slice.610), channel_id=1, source_target_pairs={{0,8},{8,16},{16,24},{24,32},{32,40},{40,48},{48,56},{56,64},{64,7... | collective-permute-start | bytes 46088 | tf_op jit(solution)/shard_map/ppermute | solution.py:30
  228.3 3.5 %fusion.102 = (f32[768]{0:T(1024)S(1)}, f32[768]{0:T(1024)S(1)}, f32[768,256]{1,0:T(8,128)S(1)}) fusion(f32[798,256]{1,0:T(8,128)S(1)} %maximum_convert_fusion.1, f32[256]{0:T(256)S(1)} %bitcast.100, f32[256]{0:T(256)S(1)} %bitcast.101, f32[256]{0:T(256)S(1)} %bitcast.144, f32[256]{0:T(256)S(1)} %bitcast.145, f32[256]{0:T(256)S(1)} %bitcast.146, ...), kind=kLoop, calls=%fused_computation.198 | loop fusion | flops 12777984 | bytes 25204736 | tf_op jit(solution)/shard_map/reduce_sum | solution.py:102
  231.9 8.9 %all_to_all.40 = f32[8,1,1536]{2,1,0:T(1,128)S(1)} all-to-all(f32[8,1,1536]{2,1,0:T(1,128)S(1)} %broadcast_in_dim.5), channel_id=1, replica_groups=mesh['sp_0'=8,'sp_1'=4,'tp'=8] {'tp'}, dimensions={0} | all-to-all | bytes 98304 | tf_op jit(solution)/shard_map/all_to_all | solution.py:35
  240.8 9.2 %all-gather.15.cloned.1.call-done = bf16[1,256,2048]{1,2,0:T(8,128)(2,1)} async-done(((bf16[1,256,256]{1,2,0:T(8,128)(2,1)}), bf16[1,256,2048]{1,2,0:T(8,128)(2,1)}) %all-gather.15.cloned.1.call-update) | async-done | bytes 1048592 | tf_op jit(solution)/shard_map/all_gather | solution.py:57
  250.1 2.3 convolution_convert_fusion
  252.4 47.2 %all_to_all.41 = bf16[8,96,2048]{2,1,0:T(8,128)(2,1)S(1)} all-to-all(bf16[8,96,2048]{2,1,0:T(8,128)(2,1)S(1)} %bitcast.97), channel_id=1, replica_groups=mesh['sp_0'=8,'sp_1'=4,'tp'=8] {'tp'}, dimensions={0} | all-to-all | bytes 6291456 | tf_op jit(solution)/shard_map/all_to_all | solution.py:69
  (81 shorter events, 9.1 us)
Async XLA Ops:
  6.5 80.6 %all-gather.9.cloned.1.call-start = ((), (), s32[]{:S(2)}) async-start(), calls=%async_computation.6 | async-start | bytes 2162688 | tf_op jit(solution)/shard_map/all_gather | solution.py:23
  13.8 6.9 %copy-start.1 = (bf16[2,256,64]{1,2,0:T(8,128)(2,1)S(1)}, bf16[2,256,64]{1,2,0:T(8,128)(2,1)}, u32[]{:S(2)}) copy-start(bf16[2,256,64]{1,2,0:T(8,128)(2,1)} %param.17) | copy-start | bytes 196612
  13.8 18.1 %copy-start.14 = (f32[2,256]{1,0:T(2,128)S(1)}, f32[2,256]{1,0:T(2,128)}, u32[]{:S(2)}) copy-start(f32[2,256]{1,0:T(2,128)} %param.14) | copy-start | bytes 6148
  13.8 18.6 %copy-start.2 = (f32[2,31,256]{2,0,1:T(2,128)S(1)}, f32[2,31,256]{2,0,1:T(2,128)}, u32[]{:S(2)}) copy-start(f32[2,31,256]{2,0,1:T(2,128)} %param.13) | copy-start | bytes 190468
  13.8 44.4 %all-to-all-start = ((bf16[8,96,2048]{2,1,0:T(8,128)(2,1)}), bf16[8,96,2048]{2,1,0:T(8,128)(2,1)S(1)}, u32[]{:S(2)}, u32[]{:S(2)}) async-start(bf16[8,96,2048]{2,1,0:T(8,128)(2,1)} %tile.4), calls=%async_computation | async-start | bytes 6291456 | tf_op jit(solution)/shard_map/all_to_all | solution.py:15
  20.7 103.4 %all-gather.13.cloned.1.call-start = ((), (), s32[]{:S(2)}) async-start(), calls=%async_computation.8 | async-start | bytes 1179648 | tf_op jit(solution)/shard_map/all_gather | solution.py:57
  87.1 2.4 copy-start.19
  89.5 3.4 %copy-start.15 = (f32[2,256]{1,0:T(2,128)S(1)}, f32[2,256]{1,0:T(2,128)}, u32[]{:S(2)}) copy-start(f32[2,256]{1,0:T(2,128)} %param.15) | copy-start | bytes 6148
  90.5 3.2 %collective-permute-start = (bf16[30,256]{1,0:T(8,128)(2,1)S(1)}, bf16[30,256]{1,0:T(8,128)(2,1)S(1)}, u32[]{:S(2)}, u32[]{:S(2)}) collective-permute-start(bf16[30,256]{1,0:T(8,128)(2,1)S(1)} %slice.576), channel_id=1, source_target_pairs={{0,8},{8,16},{16,24},{24,32},{32,40},{40,48},{48,56},{56,64},{64,7... | collective-permute-start | bytes 46088 | tf_op jit(solution)/shard_map/ppermute | solution.py:30
  93.8 14.1 %copy-start.16 = (f32[2,256]{1,0:T(2,128)S(1)}, f32[2,256]{1,0:T(2,128)}, u32[]{:S(2)}) copy-start(f32[2,256]{1,0:T(2,128)} %param.16) | copy-start | bytes 6148
  98.0 14.7 %all-to-all-start.1 = ((f32[8,1,1536]{2,1,0:T(1,128)}), f32[8,1,1536]{2,1,0:T(1,128)S(1)}, u32[]{:S(2)}, u32[]{:S(2)}) async-start(f32[8,1,1536]{2,1,0:T(1,128)} %broadcast_in_dim.4), calls=%async_computation.1 | async-start | bytes 98304 | tf_op jit(solution)/shard_map/all_to_all | solution.py:35
  128.1 47.4 %all-to-all-start.2 = ((bf16[8,96,2048]{2,1,0:T(8,128)(2,1)}), bf16[8,96,2048]{2,1,0:T(8,128)(2,1)S(1)}, u32[]{:S(2)}, u32[]{:S(2)}) async-start(bf16[8,96,2048]{2,1,0:T(8,128)(2,1)} %bitcast.96), calls=%async_computation.2 | async-start | bytes 6291456 | tf_op jit(solution)/shard_map/all_to_all | solution.py:69
  138.1 38.0 %copy-start = (bf16[96,2048]{1,0:T(8,128)(2,1)S(1)}, bf16[96,2048]{1,0:T(8,128)(2,1)}, u32[]{:S(2)}) copy-start(bf16[96,2048]{1,0:T(8,128)(2,1)} %param.9) | copy-start | bytes 1179652
  138.1 74.9 %all-gather.11.cloned.1.call-start = ((), (), s32[]{:S(2)}) async-start(), calls=%async_computation.7 | async-start | bytes 2162688 | tf_op jit(solution)/shard_map/all_gather | solution.py:23
  178.5 42.0 %all-to-all-start.3 = ((bf16[8,96,2048]{2,1,0:T(8,128)(2,1)}), bf16[8,96,2048]{2,1,0:T(8,128)(2,1)S(1)}, u32[]{:S(2)}, u32[]{:S(2)}) async-start(bf16[8,96,2048]{2,1,0:T(8,128)(2,1)} %tile.5), calls=%async_computation.3 | async-start | bytes 6291456 | tf_op jit(solution)/shard_map/all_to_all | solution.py:15
  183.0 67.0 %all-gather.15.cloned.1.call-start = ((), (), s32[]{:S(2)}) async-start(), calls=%async_computation.9 | async-start | bytes 1179648 | tf_op jit(solution)/shard_map/all_gather | solution.py:57
  220.5 2.4 copy-start.20
  222.9 5.3 %copy-start.3 = (f32[1,1,256]{2,0,1:T(1,128)S(1)}, f32[1,1,256]{2,0,1:T(1,128)}, u32[]{:S(2)}) copy-start(f32[1,1,256]{2,0,1:T(1,128)} %get-tuple-element.38) | copy-start | bytes 3076
  222.9 5.3 %copy-start.4 = (f32[1,1,256]{2,0,1:T(1,128)S(1)}, f32[1,1,256]{2,0,1:T(1,128)}, u32[]{:S(2)}) copy-start(f32[1,1,256]{2,0,1:T(1,128)} %get-tuple-element.39) | copy-start | bytes 3076
  222.9 5.3 %copy-start.5 = (f32[1,1,256]{2,0,1:T(1,128)S(1)}, f32[1,1,256]{2,0,1:T(1,128)}, u32[]{:S(2)}) copy-start(f32[1,1,256]{2,0,1:T(1,128)} %get-tuple-element.40) | copy-start | bytes 3076
  222.9 5.3 %copy-start.6 = (f32[1,1,256]{2,0,1:T(1,128)S(1)}, f32[1,1,256]{2,0,1:T(1,128)}, u32[]{:S(2)}) copy-start(f32[1,1,256]{2,0,1:T(1,128)} %get-tuple-element.41) | copy-start | bytes 3076
  222.9 5.3 %copy-start.7 = (f32[1,1,256]{2,0,1:T(1,128)S(1)}, f32[1,1,256]{2,0,1:T(1,128)}, u32[]{:S(2)}) copy-start(f32[1,1,256]{2,0,1:T(1,128)} %get-tuple-element.42) | copy-start | bytes 3076
  222.9 5.3 %copy-start.8 = (f32[1,1,256]{2,0,1:T(1,128)S(1)}, f32[1,1,256]{2,0,1:T(1,128)}, u32[]{:S(2)}) copy-start(f32[1,1,256]{2,0,1:T(1,128)} %get-tuple-element.43) | copy-start | bytes 3076
  223.0 5.3 %copy-start.9 = (f32[1,1,256]{2,0,1:T(1,128)S(1)}, f32[1,1,256]{2,0,1:T(1,128)}, u32[]{:S(2)}) copy-start(f32[1,1,256]{2,0,1:T(1,128)} %get-tuple-element.44) | copy-start | bytes 3076
  223.0 5.3 %copy-start.10 = (f32[1,1,256]{2,0,1:T(1,128)S(1)}, f32[1,1,256]{2,0,1:T(1,128)}, u32[]{:S(2)}) copy-start(f32[1,1,256]{2,0,1:T(1,128)} %get-tuple-element.45) | copy-start | bytes 3076
  223.0 5.3 %copy-start.11 = (f32[1,1,256]{2,0,1:T(1,128)S(1)}, f32[1,1,256]{2,0,1:T(1,128)}, u32[]{:S(2)}) copy-start(f32[1,1,256]{2,0,1:T(1,128)} %get-tuple-element.46) | copy-start | bytes 3076
  223.0 5.3 %copy-start.12 = (f32[1,1,256]{2,0,1:T(1,128)S(1)}, f32[1,1,256]{2,0,1:T(1,128)}, u32[]{:S(2)}) copy-start(f32[1,1,256]{2,0,1:T(1,128)} %get-tuple-element.47) | copy-start | bytes 3076
  223.0 5.3 %copy-start.13 = (f32[1,256]{1,0:T(1,128)S(1)}, f32[1,256]{1,0:T(1,128)}, u32[]{:S(2)}) copy-start(f32[1,256]{1,0:T(1,128)} %get-tuple-element.91) | copy-start | bytes 3076
  224.0 4.0 %collective-permute-start.1 = (bf16[30,256]{1,0:T(8,128)(2,1)S(1)}, bf16[30,256]{1,0:T(8,128)(2,1)S(1)}, u32[]{:S(2)}, u32[]{:S(2)}) collective-permute-start(bf16[30,256]{1,0:T(8,128)(2,1)S(1)} %slice.610), channel_id=1, source_target_pairs={{0,8},{8,16},{16,24},{24,32},{32,40},{40,48},{48,56},{56,64},{64,7... | collective-permute-start | bytes 46088 | tf_op jit(solution)/shard_map/ppermute | solution.py:30
  228.3 21.8 %copy-start.17 = (f32[1,256]{1,0:T(1,128)S(1)}, f32[1,256]{1,0:T(1,128)}, u32[]{:S(2)}) copy-start(f32[1,256]{1,0:T(1,128)} %get-tuple-element.87) | copy-start | bytes 3076
  228.3 21.8 %copy-start.18 = (f32[1,256]{1,0:T(1,128)S(1)}, f32[1,256]{1,0:T(1,128)}, u32[]{:S(2)}) copy-start(f32[1,256]{1,0:T(1,128)} %get-tuple-element.89) | copy-start | bytes 3076
Sparse Core Ops, SparseCore 0:
  9.9 77.1 all-gather.8
  88.9 35.1 all-gather.12
  141.5 71.5 all-gather.10
  214.7 35.3 all-gather.14
